TPU v7x, 32 devices: a whole 2x2x4 slice. The times are simulated.
32 devices in a mesh: rep: 2 (over x), fs: 8 (over z, y), tp: 2 (over core).
Axes of the slice: x: 2, y: 2, z: 4, core: 2. Of those that a mesh axis runs over, the one named last changes fastest.
Arguments:
- tokens: bfloat16 [16, 64, 2048], P(('rep', 'fs'), None, 'tp'), may hold values from -6 to 6
- lin_weight: bfloat16 [2048, 1024], P('fs', 'tp'), may hold values from -0.125 to 0.125
- glu_weight: bfloat16 [2048, 1024], P('fs', 'tp'), may hold values from -0.125 to 0.125
- conv_taps: float32 [31, 1024], P(None, 'tp'), may hold values from -4 to 4
- conv_gain: float32 [1024], P('tp'), may hold values from 0.1 to 1.9
- conv_out_weight: bfloat16 [1024, 2048], P('tp', 'fs'), may hold values from -0.1875 to 0.1875
- mix_gain: float32 [2048], replicated, may hold values from 0.1 to 1.9
- ff_gate: bfloat16 [2048, 5632], P('fs', 'tp'), may hold values from -0.125 to 0.125
- ff_up: bfloat16 [2048, 5632], P('fs', 'tp'), may hold values from -0.125 to 0.125
- ff_down: bfloat16 [5632, 2048], P('tp', 'fs'), may hold values from -0.078125 to 0.078125
- out_gain: float32 [2048], replicated, may hold values from 0.1 to 1.9
Outputs:
- encoded: bfloat16 [16, 64, 2048], P(('rep', 'fs'), None, 'tp')
All inputs are finite; a program needn't handle non-finite values.
Results may differ from a plain program's by a relative error of at most 0.014.
Values may be sent and summed in bfloat16 or wider, within the bound.
No kernel may reach another device: no remote copies, remote signals or barrier semaphores. Data moves between devices by JAX's collectives and lax.ppermute only.
A program may use at most 128 MiB of HBM per device.

v0:
```python
import jax
import jax.numpy as jnp
from jax import lax
from jax.sharding import PartitionSpec as P

D = 2048
CONV = 1024
TAPS = 31
residual_scale = 2.0**0.25
epsilon = 1e-05


def rounded(value):
    return lax.optimization_barrier(value.astype(jnp.bfloat16)).astype(jnp.float32)


def scaled(values, totals, squares, count):
    average = totals[:, None] / count
    second = squares[:, None] / count
    return (values - average) * lax.rsqrt(second - average * average + epsilon)


def exchange(blocks, axis):
    return lax.all_to_all(blocks, axis, 0, 0)


def after(value, *earlier):
    return lax.optimization_barrier((value, *earlier))[0]


def sum_blocks(blocks):
    return jnp.sum(blocks.astype(jnp.float32), axis=0)


def on_device(
    tokens,
    lin_weight,
    glu_weight,
    conv_taps,
    conv_gain,
    conv_out_weight,
    mix_gain,
    ff_gate,
    ff_up,
    ff_down,
    out_gain,
):
    n_fs = lax.axis_size("fs")
    n_tp = lax.axis_size("tp")
    own_tokens = tokens[0]
    seq, feat_width = own_tokens.shape
    offset = lax.axis_index("tp") * feat_width
    width = feat_width * n_tp
    rows = lin_weight.shape[0]
    chans = lin_weight.shape[1]
    units = ff_gate.shape[1] // n_fs
    all_tokens = lax.all_gather(own_tokens, "tp", axis=1, tiled=True)
    row_tokens = exchange(all_tokens.reshape(seq, n_fs, rows).transpose(1, 0, 2), "fs")
    row_tokens = row_tokens.reshape(n_fs * seq, rows)

    def dealt_columns(weight):
        blocks = weight.reshape(rows, n_fs, units).transpose(1, 0, 2)
        return exchange(blocks, "fs").reshape(n_fs * rows, units)

    gate_own = dealt_columns(after(ff_gate, row_tokens))
    up_own = dealt_columns(after(ff_up, row_tokens))
    terms = jnp.concatenate(
        [
            jnp.dot(row_tokens, lin_weight, preferred_element_type=jnp.float32),
            jnp.dot(row_tokens, glu_weight, preferred_element_type=jnp.float32),
        ],
        axis=1,
    ).astype(jnp.bfloat16)
    both = sum_blocks(exchange(terms.reshape(n_fs, seq, 2 * chans), "fs"))
    down_blocks = after(ff_down, both).reshape(n_fs, units, ff_down.shape[1])
    down_own = exchange(down_blocks, "fs").transpose(1, 0, 2).reshape(units, width)
    glu = (both[:, :chans] * jax.nn.sigmoid(both[:, chans:])).astype(jnp.bfloat16)
    margin = (TAPS - 1) // 2
    conv = lax.conv_general_dilated(
        glu.astype(jnp.float32)[None],
        conv_taps[:, None, :],
        (1,),
        [(margin, margin)],
        dimension_numbers=("NWC", "WIO", "NWC"),
        feature_group_count=glu.shape[1],
        precision=lax.Precision.HIGHEST,
    )[0]
    conv_sums, conv_squares = lax.psum((jnp.sum(conv, axis=1), jnp.sum(conv * conv, axis=1)), "tp")
    activated = jax.nn.silu(scaled(conv, conv_sums, conv_squares, CONV) * conv_gain).astype(
        jnp.bfloat16
    )
    conv_terms = jnp.dot(
        activated,
        lax.all_gather(conv_out_weight, "fs", axis=1, tiled=True),
        preferred_element_type=jnp.float32,
    )
    mixed = rounded(
        lax.psum_scatter(
            conv_terms.astype(jnp.bfloat16), "tp", scatter_dimension=1, tiled=True
        ).astype(jnp.float32)
    )
    before = residual_scale * own_tokens.astype(jnp.float32) + mixed
    mix_sums, mix_squares = lax.psum(
        (jnp.sum(before, axis=1), jnp.sum(before * before, axis=1)), "tp"
    )
    gain_own = lax.dynamic_slice_in_dim(mix_gain, offset, feat_width, 0)
    middle_own = (scaled(before, mix_sums, mix_squares, D) * gain_own).astype(jnp.bfloat16)
    middle_half = lax.all_gather(middle_own, "fs", axis=0, tiled=True)
    middle_all = lax.all_gather(middle_half, "tp", axis=1, tiled=True)
    gate = jnp.dot(middle_all, gate_own, preferred_element_type=jnp.float32)
    upward = jnp.dot(middle_all, up_own, preferred_element_type=jnp.float32)
    hidden = (jax.nn.silu(gate) * upward).astype(jnp.bfloat16)
    down_terms = jnp.dot(hidden, down_own, preferred_element_type=jnp.float32)
    halves = down_terms.astype(jnp.bfloat16).reshape(n_fs * seq, n_tp, feat_width)
    over_tp = sum_blocks(exchange(halves.transpose(1, 0, 2), "tp")).astype(jnp.bfloat16)
    over_fs = sum_blocks(exchange(over_tp.reshape(n_fs, seq, feat_width), "fs"))
    forward = rounded(over_fs)
    final = residual_scale * middle_own.astype(jnp.float32) + forward
    out_sums, out_squares = lax.psum((jnp.sum(final, axis=1), jnp.sum(final * final, axis=1)), "tp")
    gain_slice = lax.dynamic_slice_in_dim(out_gain, offset, feat_width, 0)
    encoded = (scaled(final, out_sums, out_squares, D) * gain_slice).astype(jnp.bfloat16)
    return encoded[None]


def solution(mesh):
    return jax.shard_map(
        on_device,
        mesh=mesh,
        in_specs=(
            P(("rep", "fs"), None, "tp"),
            P("fs", "tp"),
            P("fs", "tp"),
            P(None, "tp"),
            P("tp"),
            P("tp", "fs"),
            P(),
            P("fs", "tp"),
            P("fs", "tp"),
            P("tp", "fs"),
            P(),
        ),
        out_specs=P(("rep", "fs"), None, "tp"),
        check_vma=False,
    )
```

profile of v0, /device:TPU:0, one launch (start us, length us, event | category | flops | bytes accessed | tf_op | source)
XLA Modules:
  0.0 260.5 jit_solution(7943047915175370196)
XLA Ops:
  6.5 2.5 all-gather
  9.1 16.2 %all_to_all.35 = bf16[8,64,256]{2,1,0:T(8,128)(2,1)S(1)} all-to-all(bf16[8,64,256]{2,1,0:T(8,128)(2,1)S(1)} %bitcast.77), channel_id=1, replica_groups=mesh['rep'=2,'fs'=8,'tp'=2] {'fs'}, dimensions={0} | all-to-all | bytes 524288 | tf_op jit(solution)/shard_map/all_to_all | solution.py:24
  27.1 3.6 %all-to-all-start.1 = ((bf16[8,64,1024]{2,1,0:T(8,128)(2,1)}), bf16[8,64,1024]{2,1,0:T(8,128)(2,1)S(1)}, u32[]{:S(2)}, u32[]{:S(2)}) async-start(bf16[8,64,1024]{2,1,0:T(8,128)(2,1)} %pad_maximum_fusion), calls=%async_computation.1 | async-start | bytes 2097152 | tf_op jit(solution)/shard_map/all_to_all | solution.py:24
  32.9 31.7 %all-to-all-done.1 = bf16[8,64,1024]{2,1,0:T(8,128)(2,1)S(1)} async-done(((bf16[8,64,1024]{2,1,0:T(8,128)(2,1)}), bf16[8,64,1024]{2,1,0:T(8,128)(2,1)S(1)}, u32[]{:S(2)}, u32[]{:S(2)}) %all-to-all-start.1) | async-done | bytes 1048608 | tf_op jit(solution)/shard_map/all_to_all | solution.py:24
  64.7 3.6 %all-to-all-start.2 = ((bf16[8,256,352]{1,2,0:T(8,128)(2,1)}), bf16[8,256,352]{1,2,0:T(8,128)(2,1)S(1)}, u32[]{:S(2)}, u32[]{:S(2)}) async-start(bf16[8,256,352]{1,2,0:T(8,128)(2,1)} %bitcast.8), calls=%async_computation.3 | async-start | bytes 2883584 | tf_op jit(solution)/shard_map/all_to_all | solution.py:24
  68.3 2.6 copy.36
  72.5 2.5 all-reduce.2
  75.0 42.4 %all-to-all-done.2 = bf16[8,256,352]{1,2,0:T(8,128)(2,1)S(1)} async-done(((bf16[8,256,352]{1,2,0:T(8,128)(2,1)}), bf16[8,256,352]{1,2,0:T(8,128)(2,1)S(1)}, u32[]{:S(2)}, u32[]{:S(2)}) %all-to-all-start.2) | async-done | bytes 1441824 | tf_op jit(solution)/shard_map/all_to_all | solution.py:24
  117.4 3.6 %all-to-all-start.3 = ((bf16[8,256,352]{1,2,0:T(8,128)(2,1)}), bf16[8,256,352]{1,2,0:T(8,128)(2,1)S(1)}, u32[]{:S(2)}, u32[]{:S(2)}) async-start(bf16[8,256,352]{1,2,0:T(8,128)(2,1)} %bitcast.10), calls=%async_computation.4 | async-start | bytes 2883584 | tf_op jit(solution)/shard_map/all_to_all | solution.py:24
  121.1 2.9 %convolution_convert_fusion.1 = bf16[64,2048]{1,0:T(8,128)(2,1)} fusion(bf16[512,2048]{1,0:T(8,128)(2,1)} %all-gather.5.cloned.1.call-done, f32[1,64,512]{2,0,1:T(1,128)S(1)} %get-tuple-element.28, f32[512]{0:T(512)S(1)} %copy-done.7, f32[64]{0:T(128)S(1)} %get-tuple-element.26, f32[64]{0:T(128)S(1)} %get-tuple-element.25), kind=kOutput, calls=%fused_computation.1 | convolution fusion | flops 134610944 | bytes 2492928 | tf_op jit(solution)/shard_map/dot_general | solution.py:92
  124.0 9.2 %reduce-scatter.2.cloned.1.call-done = bf16[64,1024]{1,0:T(8,128)(2,1)} async-done(((bf16[64,2048]{1,0:T(8,128)(2,1)}), bf16[64,1024]{1,0:T(8,128)(2,1)}) %reduce-scatter.2.cloned.1.call-update) | async-done | bytes 131088 | tf_op jit(solution)/shard_map/reduce_scatter | solution.py:98
  134.3 2.5 all-reduce.1
  138.4 18.6 %all-to-all-done.3 = bf16[8,256,352]{1,2,0:T(8,128)(2,1)S(1)} async-done(((bf16[8,256,352]{1,2,0:T(8,128)(2,1)}), bf16[8,256,352]{1,2,0:T(8,128)(2,1)S(1)}, u32[]{:S(2)}, u32[]{:S(2)}) %all-to-all-start.3) | async-done | bytes 1441824 | tf_op jit(solution)/shard_map/all_to_all | solution.py:24
  157.0 4.3 %all-to-all-start.4 = ((bf16[8,352,256]{2,1,0:T(8,128)(2,1)}), bf16[8,352,256]{2,1,0:T(8,128)(2,1)}, u32[]{:S(2)}, u32[]{:S(2)}) async-start(bf16[8,352,256]{2,1,0:T(8,128)(2,1)} %bitcast.72), calls=%async_computation.5 | async-start | bytes 2883584 | tf_op jit(solution)/shard_map/all_to_all | solution.py:24
  161.3 25.7 %all-gather.7.cloned.1.call-done = bf16[512,1024]{1,0:T(8,128)(2,1)} async-done(((bf16[64,1024]{1,0:T(8,128)(2,1)}), bf16[512,1024]{1,0:T(8,128)(2,1)}) %all-gather.7.cloned.1.call-update) | async-done | bytes 1048592 | tf_op jit(solution)/shard_map/all_gather | solution.py:108
  189.7 13.6 %all-to-all-done.4 = bf16[8,352,256]{2,1,0:T(8,128)(2,1)} async-done(((bf16[8,352,256]{2,1,0:T(8,128)(2,1)}), bf16[8,352,256]{2,1,0:T(8,128)(2,1)}, u32[]{:S(2)}, u32[]{:S(2)}) %all-to-all-start.4) | async-done | bytes 1441824 | tf_op jit(solution)/shard_map/all_to_all | solution.py:24
  203.3 2.7 %copy.44 = bf16[8,44,8,256]{3,2,0,1:T(8,128)(2,1)} copy(bf16[8,44,8,256]{3,2,1,0:T(8,128)(2,1)} %bitcast.25) | data formatting | bytes 2883584 | tf_op jit(solution)/shard_map/reshape | solution.py:76
  205.9 2.5 fusion.31
  208.5 4.6 %convolution_convert_fusion = bf16[512,2048]{1,0:T(8,128)(2,1)S(1)} fusion(bf16[352,2048]{1,0:T(8,128)(2,1)} %bitcast.75, bf16[512,2048]{1,0:T(8,128)(2,1)} %all-gather.9.cloned.1.call-done, bf16[2048,352]{0,1:T(8,128)(2,1)} %bitcast.73, f32[512,352]{0,1:T(8,128)S(1)} %fusion.31), kind=kOutput, calls=%fused_computation | convolution fusion | flops 1478524928 | bytes 7798784 | tf_op jit(solution)/shard_map/dot_general | solution.py:113
  213.3 5.4 %all_to_all.36 = bf16[2,512,1024]{2,1,0:T(8,128)(2,1)S(1)} all-to-all(bf16[2,512,1024]{2,1,0:T(8,128)(2,1)S(1)} %bitcast.68), channel_id=1, replica_groups=mesh['rep'=2,'fs'=8,'tp'=2] {'tp'}, dimensions={0} | all-to-all | bytes 4194304 | tf_op jit(solution)/shard_map/all_to_all | solution.py:24
  218.7 1.7 reduce_sum.92
  220.4 3.7 %all-to-all-start.6 = ((bf16[8,64,1024]{2,1,0:T(8,128)(2,1)}), bf16[8,64,1024]{2,1,0:T(8,128)(2,1)S(1)}, u32[]{:S(2)}, u32[]{:S(2)}) async-start(bf16[8,64,1024]{2,1,0:T(8,128)(2,1)} %bitcast.14), calls=%async_computation.7 | async-start | bytes 2097152 | tf_op jit(solution)/shard_map/all_to_all | solution.py:24
  224.1 26.3 %all-to-all-done.6 = bf16[8,64,1024]{2,1,0:T(8,128)(2,1)S(1)} async-done(((bf16[8,64,1024]{2,1,0:T(8,128)(2,1)}), bf16[8,64,1024]{2,1,0:T(8,128)(2,1)S(1)}, u32[]{:S(2)}, u32[]{:S(2)}) %all-to-all-start.6) | async-done | bytes 1048608 | tf_op jit(solution)/shard_map/all_to_all | solution.py:24
  250.7 2.5 all-reduce
  (52 shorter events, 12.6 us)
Async XLA Ops:
  6.5 18.8 %copy-start = (bf16[256,512]{1,0:T(8,128)(2,1)S(1)}, bf16[256,512]{1,0:T(8,128)(2,1)}, u32[]{:S(2)}) copy-start(bf16[256,512]{1,0:T(8,128)(2,1)} %param.13) | copy-start | bytes 786436
  6.5 19.1 %copy-start.5 = (bf16[256,512]{1,0:T(8,128)(2,1)S(1)}, bf16[256,512]{1,0:T(8,128)(2,1)}, u32[]{:S(2)}) copy-start(bf16[256,512]{1,0:T(8,128)(2,1)} %param.12) | copy-start | bytes 786436
  25.9 5.5 %copy-start.2 = (bf16[256,2816]{1,0:T(8,128)(2,1)S(1)}, bf16[256,2816]{1,0:T(8,128)(2,1)}, u32[]{:S(2)}) copy-start(bf16[256,2816]{1,0:T(8,128)(2,1)} %param.18) | copy-start | bytes 4325380
  27.1 37.6 %all-to-all-start.1 = ((bf16[8,64,1024]{2,1,0:T(8,128)(2,1)}), bf16[8,64,1024]{2,1,0:T(8,128)(2,1)S(1)}, u32[]{:S(2)}, u32[]{:S(2)}) async-start(bf16[8,64,1024]{2,1,0:T(8,128)(2,1)} %pad_maximum_fusion), calls=%async_computation.1 | async-start | bytes 2097152 | tf_op jit(solution)/shard_map/all_to_all | solution.py:24
  30.6 90.4 %all-gather.5.cloned.1.call-start = ((), (), s32[]{:S(2)}) async-start(), calls=%async_computation.8 | async-start | bytes 2359296 | tf_op jit(solution)/shard_map/all_gather | solution.py:94
  64.7 52.7 %all-to-all-start.2 = ((bf16[8,256,352]{1,2,0:T(8,128)(2,1)}), bf16[8,256,352]{1,2,0:T(8,128)(2,1)S(1)}, u32[]{:S(2)}, u32[]{:S(2)}) async-start(bf16[8,256,352]{1,2,0:T(8,128)(2,1)} %bitcast.8), calls=%async_computation.3 | async-start | bytes 2883584 | tf_op jit(solution)/shard_map/all_to_all | solution.py:24
  68.3 2.8 %copy-start.8 = (f32[31,512]{1,0:T(8,128)S(1)}, f32[31,512]{1,0:T(8,128)}, u32[]{:S(2)}) copy-start(f32[31,512]{1,0:T(8,128)} %param.14) | copy-start | bytes 190468
  71.1 50.0 %copy-start.7 = (f32[512]{0:T(512)S(1)}, f32[512]{0:T(512)}, u32[]{:S(2)}) copy-start(f32[512]{0:T(512)} %param.15) | copy-start | bytes 6148
  117.4 39.6 %all-to-all-start.3 = ((bf16[8,256,352]{1,2,0:T(8,128)(2,1)}), bf16[8,256,352]{1,2,0:T(8,128)(2,1)S(1)}, u32[]{:S(2)}, u32[]{:S(2)}) async-start(bf16[8,256,352]{1,2,0:T(8,128)(2,1)} %bitcast.10), calls=%async_computation.4 | async-start | bytes 2883584 | tf_op jit(solution)/shard_map/all_to_all | solution.py:24
  121.0 3.0 %copy-start.6 = (f32[2048]{0:T(1024)S(1)}, f32[2048]{0:T(1024)}, u32[]{:S(2)}) copy-start(f32[2048]{0:T(1024)} %param.17) | copy-start | bytes 24580
  121.0 12.2 %copy-start.4 = (bf16[1,64,1024]{2,1,0:T(8,128)(2,1)S(1)}, bf16[1,64,1024]{2,1,0:T(8,128)(2,1)}, u32[]{:S(2)}) copy-start(bf16[1,64,1024]{2,1,0:T(8,128)(2,1)} %param.11) | copy-start | bytes 393220
  121.0 12.2 %reduce-scatter.2.cloned.1.call-start = ((), (), s32[]{:S(2)}) async-start(), calls=%async_computation.9 | async-start | bytes 393216 | tf_op jit(solution)/shard_map/reduce_scatter | solution.py:98
  123.9 63.2 %all-gather.7.cloned.1.call-start = ((), (), s32[]{:S(2)}) async-start(), calls=%async_computation.10 | async-start | bytes 1179648 | tf_op jit(solution)/shard_map/all_gather | solution.py:108
  157.0 46.3 %all-to-all-start.4 = ((bf16[8,352,256]{2,1,0:T(8,128)(2,1)}), bf16[8,352,256]{2,1,0:T(8,128)(2,1)}, u32[]{:S(2)}, u32[]{:S(2)}) async-start(bf16[8,352,256]{2,1,0:T(8,128)(2,1)} %bitcast.72), calls=%async_computation.5 | async-start | bytes 2883584 | tf_op jit(solution)/shard_map/all_to_all | solution.py:24
  161.3 44.6 %all-gather.9.cloned.1.call-start = ((), (), s32[]{:S(2)}) async-start(), calls=%async_computation.11 | async-start | bytes 3145728 | tf_op jit(solution)/shard_map/all_gather | solution.py:109
  189.7 16.2 %copy-start.3 = (bf16[8,44,8,256]{3,2,0,1:T(8,128)(2,1)S(1)}, bf16[8,44,8,256]{3,2,0,1:T(8,128)(2,1)}, u32[]{:S(2)}) copy-start(bf16[8,44,8,256]{3,2,0,1:T(8,128)(2,1)} %copy.42) | copy-start | bytes 4325380
  220.4 30.1 %copy-start.1 = (bf16[64,1024]{1,0:T(8,128)(2,1)S(1)}, bf16[64,1024]{1,0:T(8,128)(2,1)}, u32[]{:S(2)}) copy-start(bf16[64,1024]{1,0:T(8,128)(2,1)} %multiply_convert_fusion.1) | copy-start | bytes 393220
  220.4 32.8 %dynamic-slice-start = ((f32[2048]{0:T(1024)}, s32[]{:T(128)}), f32[1024]{0:T(1024)S(1)}, s32[]{:S(2)}) async-start(f32[2048]{0:T(1024)} %param.21, s32[]{:T(128)} %select_n.4), calls=%async_computation.12 | async-start | bytes 8704 | tf_op jit(solution)/shard_map/dynamic_slice | solution.py:120
  220.4 30.0 %all-to-all-start.6 = ((bf16[8,64,1024]{2,1,0:T(8,128)(2,1)}), bf16[8,64,1024]{2,1,0:T(8,128)(2,1)S(1)}, u32[]{:S(2)}, u32[]{:S(2)}) async-start(bf16[8,64,1024]{2,1,0:T(8,128)(2,1)} %bitcast.14), calls=%async_computation.7 | async-start | bytes 2097152 | tf_op jit(solution)/shard_map/all_to_all | solution.py:24
Sparse Core Ops, SparseCore 0:
  33.5 80.9 all-gather.4
  124.1 9.0 reduce-scatter.1
  138.5 48.5 all-gather.6
  188.5 14.5 all-gather.8
where the time goes:
time: 261 us; the launch traced here: 260 us
  waiting for transfers between devices  168 us (64%)
  blocking collectives  31.5 us (12%)
  starting transfers between devices  18.9 us (7%)
  between operations  13.4 us (5%)
  matrix products  11.9 us (5%)
  local copies, waits for them, and re-layouts  9.7 us (4%)
  other arithmetic  7.01 us (3%)
    all_to_all x5, waiting for transfers between devices, exchange(): return lax.all_to_all(blocks, axis, 0, 0)  132 us
    all_gather x1, waiting for transfers between devices, on_device(): middle_half = lax.all_gather(middle_own, 'fs', axis=0, tiled=True)  25.7 us
    all_to_all x2, blocking collectives, exchange(): return lax.all_to_all(blocks, axis, 0, 0)  21.6 us
    all_to_all x5, starting transfers between devices, exchange(): return lax.all_to_all(blocks, axis, 0, 0)  18.7 us
    reduce_scatter x1, waiting for transfers between devices, on_device(): lax.psum_scatter(conv_terms.astype(jnp.bfloat16), 'tp', scatter_dimension...  9.16 us
  transfers between devices with their start and end apart: 9, of which 7 were waited for; matrix products, arithmetic and copies ran while one was open for 6% of the time, Pallas kernels for 0%

commit v1 on v0

--- a/solution.py
+++ b/solution.py
@@ -106,7 +106,7 @@
     gain_own = lax.dynamic_slice_in_dim(mix_gain, offset, feat_width, 0)
     middle_own = (scaled(before, mix_sums, mix_squares, D) * gain_own).astype(jnp.bfloat16)
     middle_half = lax.all_gather(middle_own, "fs", axis=0, tiled=True)
-    middle_all = lax.all_gather(middle_half, "tp", axis=1, tiled=True)
+    middle_all = jnp.concatenate(lax.all_gather(middle_half, "tp"), axis=1)
     gate = jnp.dot(middle_all, gate_own, preferred_element_type=jnp.float32)
     upward = jnp.dot(middle_all, up_own, preferred_element_type=jnp.float32)
     hidden = (jax.nn.silu(gate) * upward).astype(jnp.bfloat16)

time: 261 us -> 266 us (1.019)
  local copies, waits for them, and re-layouts: 9.7 us -> 14.2 us
    all_gather x0 -> x1, local copies, waits for them, and re-layouts: none -> 2.85 us  [on_device(): middle_all = jnp.concatenate(lax.all_gather(middle_half, 'tp'), axis=1)]
where the time goes in v1:
time: 266 us; the launch traced here: 265 us
  waiting for transfers between devices  168 us (63%)
  blocking collectives  31.5 us (12%)
  starting transfers between devices  19 us (7%)
  local copies, waits for them, and re-layouts  14.2 us (5%)
  between operations  13.3 us (5%)
  matrix products  12.3 us (5%)
  other arithmetic  7.02 us (3%)
    all_to_all x5, waiting for transfers between devices, exchange(): return lax.all_to_all(blocks, axis, 0, 0)  132 us
    all_gather x1, waiting for transfers between devices, on_device(): middle_half = lax.all_gather(middle_own, 'fs', axis=0, tiled=True)  26 us
    all_to_all x2, blocking collectives, exchange(): return lax.all_to_all(blocks, axis, 0, 0)  21.6 us
    all_to_all x5, starting transfers between devices, exchange(): return lax.all_to_all(blocks, axis, 0, 0)  18.8 us
    reduce_scatter x1, waiting for transfers between devices, on_device(): lax.psum_scatter(conv_terms.astype(jnp.bfloat16), 'tp', scatter_dimension...  9.16 us
  transfers between devices with their start and end apart: 9, of which 7 were waited for; matrix products, arithmetic and copies ran while one was open for 6% of the time, Pallas kernels for 0%

profile of v1, /device:TPU:0, one launch (start us, length us, event | category | flops | bytes accessed | tf_op | source)
XLA Modules:
  0.0 265.3 jit_solution(6308224283904223196)
XLA Ops:
  6.5 2.5 all-gather
  9.1 16.2 %all_to_all.35 = bf16[8,64,256]{2,1,0:T(8,128)(2,1)S(1)} all-to-all(bf16[8,64,256]{2,1,0:T(8,128)(2,1)S(1)} %bitcast.84), channel_id=1, replica_groups=mesh['rep'=2,'fs'=8,'tp'=2] {'fs'}, dimensions={0} | all-to-all | bytes 524288 | tf_op jit(solution)/shard_map/all_to_all | solution.py:24
  27.1 3.6 %all-to-all-start.1 = ((bf16[8,64,1024]{2,1,0:T(8,128)(2,1)}), bf16[8,64,1024]{2,1,0:T(8,128)(2,1)S(1)}, u32[]{:S(2)}, u32[]{:S(2)}) async-start(bf16[8,64,1024]{2,1,0:T(8,128)(2,1)} %pad_maximum_fusion), calls=%async_computation.1 | async-start | bytes 2097152 | tf_op jit(solution)/shard_map/all_to_all | solution.py:24
  33.0 31.7 %all-to-all-done.1 = bf16[8,64,1024]{2,1,0:T(8,128)(2,1)S(1)} async-done(((bf16[8,64,1024]{2,1,0:T(8,128)(2,1)}), bf16[8,64,1024]{2,1,0:T(8,128)(2,1)S(1)}, u32[]{:S(2)}, u32[]{:S(2)}) %all-to-all-start.1) | async-done | bytes 1048608 | tf_op jit(solution)/shard_map/all_to_all | solution.py:24
  64.7 3.6 %all-to-all-start.2 = ((bf16[8,256,352]{1,2,0:T(8,128)(2,1)}), bf16[8,256,352]{1,2,0:T(8,128)(2,1)S(1)}, u32[]{:S(2)}, u32[]{:S(2)}) async-start(bf16[8,256,352]{1,2,0:T(8,128)(2,1)} %bitcast.11), calls=%async_computation.3 | async-start | bytes 2883584 | tf_op jit(solution)/shard_map/all_to_all | solution.py:24
  68.3 2.6 copy.39
  72.5 2.5 all-reduce.2
  75.0 42.4 %all-to-all-done.2 = bf16[8,256,352]{1,2,0:T(8,128)(2,1)S(1)} async-done(((bf16[8,256,352]{1,2,0:T(8,128)(2,1)}), bf16[8,256,352]{1,2,0:T(8,128)(2,1)S(1)}, u32[]{:S(2)}, u32[]{:S(2)}) %all-to-all-start.2) | async-done | bytes 1441824 | tf_op jit(solution)/shard_map/all_to_all | solution.py:24
  117.4 3.6 %all-to-all-start.3 = ((bf16[8,256,352]{1,2,0:T(8,128)(2,1)}), bf16[8,256,352]{1,2,0:T(8,128)(2,1)S(1)}, u32[]{:S(2)}, u32[]{:S(2)}) async-start(bf16[8,256,352]{1,2,0:T(8,128)(2,1)} %bitcast.14), calls=%async_computation.4 | async-start | bytes 2883584 | tf_op jit(solution)/shard_map/all_to_all | solution.py:24
  121.1 2.8 %convolution_convert_fusion.1 = bf16[64,2048]{1,0:T(8,128)(2,1)} fusion(bf16[512,2048]{1,0:T(8,128)(2,1)} %all-gather.6.cloned.1.call-done, f32[1,64,512]{2,0,1:T(1,128)S(1)} %get-tuple-element.28, f32[512]{0:T(512)S(1)} %copy-done.6, f32[64]{0:T(128)S(1)} %get-tuple-element.26, f32[64]{0:T(128)S(1)} %get-tuple-element.25), kind=kOutput, calls=%fused_computation.1 | convolution fusion | flops 134610944 | bytes 2492928 | tf_op jit(solution)/shard_map/dot_general | solution.py:92
  124.0 9.2 %reduce-scatter.2.cloned.1.call-done = bf16[64,1024]{1,0:T(8,128)(2,1)} async-done(((bf16[64,2048]{1,0:T(8,128)(2,1)}), bf16[64,1024]{1,0:T(8,128)(2,1)}) %reduce-scatter.2.cloned.1.call-update) | async-done | bytes 131088 | tf_op jit(solution)/shard_map/reduce_scatter | solution.py:98
  134.2 2.5 all-reduce.1
  138.4 18.6 %all-to-all-done.3 = bf16[8,256,352]{1,2,0:T(8,128)(2,1)S(1)} async-done(((bf16[8,256,352]{1,2,0:T(8,128)(2,1)}), bf16[8,256,352]{1,2,0:T(8,128)(2,1)S(1)}, u32[]{:S(2)}, u32[]{:S(2)}) %all-to-all-start.3) | async-done | bytes 1441824 | tf_op jit(solution)/shard_map/all_to_all | solution.py:24
  157.0 4.3 %all-to-all-start.4 = ((bf16[8,352,256]{2,1,0:T(8,128)(2,1)}), bf16[8,352,256]{2,1,0:T(8,128)(2,1)}, u32[]{:S(2)}, u32[]{:S(2)}) async-start(bf16[8,352,256]{2,1,0:T(8,128)(2,1)} %bitcast.79), calls=%async_computation.5 | async-start | bytes 2883584 | tf_op jit(solution)/shard_map/all_to_all | solution.py:24
  161.3 26.0 %all-gather.8.cloned.1.call-done = bf16[512,1024]{1,0:T(8,128)(2,1)} async-done(((bf16[64,1024]{1,0:T(8,128)(2,1)}), bf16[512,1024]{1,0:T(8,128)(2,1)}) %all-gather.8.cloned.1.call-update) | async-done | bytes 1048592 | tf_op jit(solution)/shard_map/all_gather | solution.py:108
  189.9 13.3 %all-to-all-done.4 = bf16[8,352,256]{2,1,0:T(8,128)(2,1)} async-done(((bf16[8,352,256]{2,1,0:T(8,128)(2,1)}), bf16[8,352,256]{2,1,0:T(8,128)(2,1)}, u32[]{:S(2)}, u32[]{:S(2)}) %all-to-all-start.4) | async-done | bytes 1441824 | tf_op jit(solution)/shard_map/all_to_all | solution.py:24
  203.3 2.6 copy.47
  205.9 2.9 %copy.36 = bf16[2,512,1024]{1,2,0:T(8,128)(2,1)S(1)} copy(bf16[2,512,1024]{2,1,0:T(8,128)(2,1)} %bitcast.75) | data formatting | bytes 4194304 | tf_op jit(solution)/shard_map/all_gather | solution.py:109
  208.8 2.3 fusion.31
  211.0 5.3 %convolution_convert_fusion = bf16[512,2048]{1,0:T(8,128)(2,1)} fusion(bf16[352,2048]{1,0:T(8,128)(2,1)} %bitcast.82, bf16[2048,352]{0,1:T(8,128)(2,1)} %bitcast.81, bf16[512,2048]{0,1:T(8,128)(2,1)S(1)} %bitcast.77, f32[512,352]{0,1:T(8,128)S(1)} %fusion.31), kind=kOutput, calls=%fused_computation | convolution fusion | flops 1478524928 | bytes 7798784 | tf_op jit(solution)/shard_map/dot_general | solution.py:113
  218.1 5.4 %all_to_all.36 = bf16[2,512,1024]{2,1,0:T(8,128)(2,1)S(1)} all-to-all(bf16[2,512,1024]{2,1,0:T(8,128)(2,1)S(1)} %bitcast.72), channel_id=1, replica_groups=mesh['rep'=2,'fs'=8,'tp'=2] {'tp'}, dimensions={0} | all-to-all | bytes 4194304 | tf_op jit(solution)/shard_map/all_to_all | solution.py:24
  225.2 3.8 %all-to-all-start.6 = ((bf16[8,64,1024]{2,1,0:T(8,128)(2,1)}), bf16[8,64,1024]{2,1,0:T(8,128)(2,1)S(1)}, u32[]{:S(2)}, u32[]{:S(2)}) async-start(bf16[8,64,1024]{2,1,0:T(8,128)(2,1)} %bitcast.18), calls=%async_computation.7 | async-start | bytes 2097152 | tf_op jit(solution)/shard_map/all_to_all | solution.py:24
  229.1 26.1 %all-to-all-done.6 = bf16[8,64,1024]{2,1,0:T(8,128)(2,1)S(1)} async-done(((bf16[8,64,1024]{2,1,0:T(8,128)(2,1)}), bf16[8,64,1024]{2,1,0:T(8,128)(2,1)S(1)}, u32[]{:S(2)}, u32[]{:S(2)}) %all-to-all-start.6) | async-done | bytes 1048608 | tf_op jit(solution)/shard_map/all_to_all | solution.py:24
  255.5 2.5 all-reduce
  (51 shorter events, 15.9 us)
Async XLA Ops:
  6.5 18.8 %copy-start = (bf16[256,512]{1,0:T(8,128)(2,1)S(1)}, bf16[256,512]{1,0:T(8,128)(2,1)}, u32[]{:S(2)}) copy-start(bf16[256,512]{1,0:T(8,128)(2,1)} %param.13) | copy-start | bytes 786436
  6.5 19.1 %copy-start.4 = (bf16[256,512]{1,0:T(8,128)(2,1)S(1)}, bf16[256,512]{1,0:T(8,128)(2,1)}, u32[]{:S(2)}) copy-start(bf16[256,512]{1,0:T(8,128)(2,1)} %param.12) | copy-start | bytes 786436
  25.9 5.5 %copy-start.2 = (bf16[256,2816]{1,0:T(8,128)(2,1)S(1)}, bf16[256,2816]{1,0:T(8,128)(2,1)}, u32[]{:S(2)}) copy-start(bf16[256,2816]{1,0:T(8,128)(2,1)} %param.18) | copy-start | bytes 4325380
  27.1 37.6 %all-to-all-start.1 = ((bf16[8,64,1024]{2,1,0:T(8,128)(2,1)}), bf16[8,64,1024]{2,1,0:T(8,128)(2,1)S(1)}, u32[]{:S(2)}, u32[]{:S(2)}) async-start(bf16[8,64,1024]{2,1,0:T(8,128)(2,1)} %pad_maximum_fusion), calls=%async_computation.1 | async-start | bytes 2097152 | tf_op jit(solution)/shard_map/all_to_all | solution.py:24
  30.7 90.4 %all-gather.6.cloned.1.call-start = ((), (), s32[]{:S(2)}) async-start(), calls=%async_computation.8 | async-start | bytes 2359296 | tf_op jit(solution)/shard_map/all_gather | solution.py:94
  64.7 52.7 %all-to-all-start.2 = ((bf16[8,256,352]{1,2,0:T(8,128)(2,1)}), bf16[8,256,352]{1,2,0:T(8,128)(2,1)S(1)}, u32[]{:S(2)}, u32[]{:S(2)}) async-start(bf16[8,256,352]{1,2,0:T(8,128)(2,1)} %bitcast.11), calls=%async_computation.3 | async-start | bytes 2883584 | tf_op jit(solution)/shard_map/all_to_all | solution.py:24
  68.3 2.8 %copy-start.7 = (f32[31,512]{1,0:T(8,128)S(1)}, f32[31,512]{1,0:T(8,128)}, u32[]{:S(2)}) copy-start(f32[31,512]{1,0:T(8,128)} %param.14) | copy-start | bytes 190468
  71.1 50.0 %copy-start.6 = (f32[512]{0:T(512)S(1)}, f32[512]{0:T(512)}, u32[]{:S(2)}) copy-start(f32[512]{0:T(512)} %param.15) | copy-start | bytes 6148
  117.4 39.6 %all-to-all-start.3 = ((bf16[8,256,352]{1,2,0:T(8,128)(2,1)}), bf16[8,256,352]{1,2,0:T(8,128)(2,1)S(1)}, u32[]{:S(2)}, u32[]{:S(2)}) async-start(bf16[8,256,352]{1,2,0:T(8,128)(2,1)} %bitcast.14), calls=%async_computation.4 | async-start | bytes 2883584 | tf_op jit(solution)/shard_map/all_to_all | solution.py:24
  121.0 3.0 %copy-start.5 = (f32[2048]{0:T(1024)S(1)}, f32[2048]{0:T(1024)}, u32[]{:S(2)}) copy-start(f32[2048]{0:T(1024)} %param.17) | copy-start | bytes 24580
  121.0 12.2 %copy-start.3 = (bf16[1,64,1024]{2,1,0:T(8,128)(2,1)S(1)}, bf16[1,64,1024]{2,1,0:T(8,128)(2,1)}, u32[]{:S(2)}) copy-start(bf16[1,64,1024]{2,1,0:T(8,128)(2,1)} %param.11) | copy-start | bytes 393220
  121.0 12.2 %reduce-scatter.2.cloned.1.call-start = ((), (), s32[]{:S(2)}) async-start(), calls=%async_computation.9 | async-start | bytes 393216 | tf_op jit(solution)/shard_map/reduce_scatter | solution.py:98
  123.9 63.4 %all-gather.8.cloned.1.call-start = ((), (), s32[]{:S(2)}) async-start(), calls=%async_computation.10 | async-start | bytes 1179648 | tf_op jit(solution)/shard_map/all_gather | solution.py:108
  157.0 46.2 %all-to-all-start.4 = ((bf16[8,352,256]{2,1,0:T(8,128)(2,1)}), bf16[8,352,256]{2,1,0:T(8,128)(2,1)}, u32[]{:S(2)}, u32[]{:S(2)}) async-start(bf16[8,352,256]{2,1,0:T(8,128)(2,1)} %bitcast.79), calls=%async_computation.5 | async-start | bytes 2883584 | tf_op jit(solution)/shard_map/all_to_all | solution.py:24
  161.3 44.6 %all-gather.10.cloned.1.call-start = ((), (), s32[]{:S(2)}) async-start(), calls=%async_computation.11 | async-start | bytes 3145728 | tf_op jit(solution)/shard_map/all_gather | solution.py:109
  225.2 30.1 %copy-start.1 = (bf16[64,1024]{1,0:T(8,128)(2,1)S(1)}, bf16[64,1024]{1,0:T(8,128)(2,1)}, u32[]{:S(2)}) copy-start(bf16[64,1024]{1,0:T(8,128)(2,1)} %multiply_convert_fusion.1) | copy-start | bytes 393220
  225.2 32.8 %dynamic-slice-start = ((f32[2048]{0:T(1024)}, s32[]{:T(128)}), f32[1024]{0:T(1024)S(1)}, s32[]{:S(2)}) async-start(f32[2048]{0:T(1024)} %param.21, s32[]{:T(128)} %select_n.4), calls=%async_computation.12 | async-start | bytes 8704 | tf_op jit(solution)/shard_map/dynamic_slice | solution.py:120
  225.2 30.0 %all-to-all-start.6 = ((bf16[8,64,1024]{2,1,0:T(8,128)(2,1)}), bf16[8,64,1024]{2,1,0:T(8,128)(2,1)S(1)}, u32[]{:S(2)}, u32[]{:S(2)}) async-start(bf16[8,64,1024]{2,1,0:T(8,128)(2,1)} %bitcast.18), calls=%async_computation.7 | async-start | bytes 2097152 | tf_op jit(solution)/shard_map/all_to_all | solution.py:24
Sparse Core Ops, SparseCore 0:
  33.5 80.9 all-gather.5
  124.1 9.0 reduce-scatter.1
  138.5 48.7 all-gather.7
  188.7 14.4 all-gather.9
